TPU v7x, 256 devices: a whole 4x4x8 slice. The times are simulated.
256 devices in a mesh: ep: 32 (over z, x), tp: 8 (over y, core).
Axes of the slice: x: 4, y: 4, z: 8, core: 2. Of those that a mesh axis runs over, the one named last changes fastest.
Arguments:
- queries: bfloat16 [4096, 4096], P('ep', 'tp'), may hold values from -6 to 6
- key_rows: bfloat16 [4096, 4096], P('ep', 'tp'), may hold values from -6 to 6
- value_rows: bfloat16 [4096, 4096], P('ep', 'tp'), may hold values from -6 to 6
- key_shift: bfloat16 [4096, 64], P('ep', 'tp'), may hold values from -20 to 1
- out_weight: bfloat16 [4096, 4096], P('tp'), may hold values from -0.09375 to 0.09375
- routed_rows: bfloat16 [4096, 4096], P('ep'), may hold values from -6 to 6
- expert_ids: int32 [4096, 2], P('ep'), may hold values from 0 to 31, as said below
- route_weights: float32 [4096, 2], P(('ep', 'tp')), may hold values from 0.2 to 1
- gate_weight: bfloat16 [32, 4096, 1024], P('ep', None, 'tp'), may hold values from -0.09375 to 0.09375
- up_weight: bfloat16 [32, 4096, 1024], P('ep', None, 'tp'), may hold values from -0.09375 to 0.09375
- down_weight: bfloat16 [32, 1024, 4096], P('ep', 'tp'), may hold values from -0.1875 to 0.1875
Outputs:
- mixed_rows: bfloat16 [4096, 4096], P(('ep', 'tp'))
- routed_out: bfloat16 [4096, 4096], P(('ep', 'tp'))
Inputs may be any that keep to these rules, and one draw needn't show every extreme that they name: `expert_ids`: the two ids of a token differ and lie in one group of 8 consecutive experts. Within each aligned block of 16 tokens no expert is named more than 2 times.
All inputs are finite; a program needn't handle non-finite values.
Results may differ from a plain program's by a relative error of at most 0.015.
Values may be sent and summed in bfloat16 or wider, within the bound.
No kernel may reach another device: no remote copies, remote signals or barrier semaphores. Data moves between devices by JAX's collectives and lax.ppermute only.
A program may use at most 128 MiB of HBM per device.

v0:
```python
import jax
import jax.numpy as jnp
from jax import lax
from jax.sharding import PartitionSpec as P

HEAD = 64
KEY_BLOCK = 512


def sent_together(arrays, axis, dim, along):
    both = jnp.concatenate(arrays, axis=along)
    result, at, finished = (lax.all_gather(both, axis, axis=dim, tiled=True), 0, [])
    for a in arrays:
        finished.append(lax.slice_in_dim(result, at, at + a.shape[along], axis=along))
        at += a.shape[along]
    return tuple(finished)


def in_blocks(value, dim, peers):
    before, after = (value.shape[:dim], value.shape[dim + 1 :])
    return jnp.moveaxis(value.reshape(*before, peers, -1, *after), dim, 0)


def sent_and_summed(value, axis, dim):
    tiles = in_blocks(value, dim, lax.axis_size(axis))
    arrived = lax.all_to_all(tiles, axis, split_axis=0, concat_axis=0, tiled=True)
    return arrived.astype(jnp.float32).sum(axis=0)


def stick_attend(query_rows, key_all, value_all, shift_all, first_pos):
    row_count = query_rows.shape[0]
    head_count = query_rows.shape[1]
    head_depth = query_rows.shape[2]
    query_pos = first_pos + jnp.arange(row_count, dtype=jnp.int32)
    last_block = (first_pos + row_count - 1) // KEY_BLOCK
    score_scale = head_depth ** (-0.5)

    def sweep_block(step_index, state_pair):
        running, logsum = state_pair
        row_start = (last_block - step_index) * KEY_BLOCK
        key_tile_block = lax.dynamic_slice_in_dim(key_all, row_start, KEY_BLOCK, 0).reshape(
            KEY_BLOCK, head_count, head_depth
        )
        value_block = lax.dynamic_slice_in_dim(value_all, row_start, KEY_BLOCK, 0).reshape(
            KEY_BLOCK, head_count, head_depth
        )
        shift_block = lax.dynamic_slice_in_dim(shift_all, row_start, KEY_BLOCK, 0).astype(
            jnp.float32
        )
        scores = (
            jnp.einsum(
                "thd,shd->hts", query_rows, key_tile_block, preferred_element_type=jnp.float32
            )
            * score_scale
        )
        scores = scores + shift_block.T[:, None, :]
        key_pos = row_start + jnp.arange(KEY_BLOCK, dtype=jnp.int32)
        strict = (key_pos[None, :] < query_pos[:, None])[None]
        log_keep = jnp.where(strict, jax.nn.log_sigmoid(-scores), 0.0)
        suffix = lax.cumsum(log_keep, axis=2, reverse=True) - log_keep + logsum[:, :, None]
        weight = jnp.where(strict, jnp.exp(jax.nn.log_sigmoid(scores) + suffix), 0.0).astype(
            jnp.bfloat16
        )
        running = running + jnp.einsum(
            "hts,shd->htd", weight, value_block, preferred_element_type=jnp.float32
        )
        return (running, logsum + jnp.sum(log_keep, axis=2))

    initial = (
        jnp.zeros((head_count, row_count, head_depth), jnp.float32),
        jnp.zeros((head_count, row_count), jnp.float32),
    )
    running, logsum = lax.fori_loop(0, last_block + 1, sweep_block, initial)
    return (
        jnp.transpose(running, (1, 0, 2))
        .reshape(row_count, head_count * head_depth)
        .astype(jnp.bfloat16)
    )


def slot_numbers(pair_ids, expert_count):
    one_hot = (pair_ids[..., None] == jnp.arange(expert_count, dtype=jnp.int32)).astype(jnp.int32)
    earlier = jnp.cumsum(one_hot, axis=1) - one_hot
    return jnp.sum(one_hot * earlier, axis=2)


def pack_rows(source_rows, destination, slot_count):
    pair_count = destination.shape[0]
    matches = destination[None, :] == jnp.arange(slot_count, dtype=jnp.int32)[:, None]
    source_index = jnp.sum(
        jnp.where(matches, jnp.arange(pair_count, dtype=jnp.int32)[None, :] // 2, 0), axis=1
    )
    filled = jnp.any(matches, axis=1)
    picked = jnp.take(source_rows, source_index, axis=0)
    return jnp.where(filled[:, None], picked, jnp.zeros_like(picked))


def expand(expert_rows, gate_part, up_part):
    gate_proj = jnp.einsum(
        "rcd,df->rcf", expert_rows, gate_part, preferred_element_type=jnp.float32
    )
    up_proj = jnp.einsum("rcd,df->rcf", expert_rows, up_part, preferred_element_type=jnp.float32)
    return (jax.nn.silu(gate_proj) * up_proj).astype(jnp.bfloat16)


def shards(
    queries,
    key_rows,
    value_rows,
    key_shift,
    out_weight,
    routed_rows,
    expert_ids,
    route_weights,
    gate_weight,
    up_weight,
    down_weight,
):
    tp_count = lax.axis_size("tp")
    local_rows = queries.shape[0]
    heads_here = key_shift.shape[1]
    key_all, value_all, shift_all = sent_together((key_rows, value_rows, key_shift), "ep", 0, 1)
    first_pos = lax.axis_index("ep") * local_rows
    attended = stick_attend(
        queries.reshape(local_rows, heads_here, HEAD), key_all, value_all, shift_all, first_pos
    )
    mixed_rows = sent_and_summed(
        jnp.dot(attended, out_weight, preferred_element_type=jnp.float32).astype(jnp.bfloat16),
        "tp",
        0,
    ).astype(jnp.bfloat16)
    expert_count = lax.axis_size("ep")
    sub_rows = local_rows // tp_count
    capacity = 4 * sub_rows // expert_count
    model_width = routed_rows.shape[1]
    column = lax.axis_index("tp")
    own_ids = lax.dynamic_slice_in_dim(expert_ids, column * sub_rows, sub_rows, 0).reshape(
        1, sub_rows * 2
    )
    own_slot = slot_numbers(own_ids, expert_count)[0]
    own_dest = own_ids[0] * capacity + own_slot
    own_input = lax.dynamic_slice_in_dim(routed_rows, column * sub_rows, sub_rows, 0)
    outgoing = pack_rows(own_input, own_dest, expert_count * capacity).reshape(
        expert_count, capacity, model_width
    )
    arrived = lax.all_to_all(outgoing, "ep", split_axis=0, concat_axis=0, tiled=True)
    hidden = expand(lax.all_gather(arrived, "tp", axis=1, tiled=True), gate_weight[0], up_weight[0])
    unit_count = hidden.shape[2]
    ordered = jnp.transpose(
        hidden.reshape(expert_count, tp_count, capacity, unit_count), (1, 0, 2, 3)
    )
    ordered = ordered.reshape(tp_count * expert_count * capacity, unit_count)
    partial_value = sent_and_summed(
        jnp.dot(ordered, down_weight[0], preferred_element_type=jnp.float32).astype(jnp.bfloat16),
        "tp",
        0,
    ).astype(jnp.bfloat16)
    returned = lax.all_to_all(
        partial_value.reshape(expert_count, capacity, model_width),
        "ep",
        split_axis=0,
        concat_axis=0,
        tiled=True,
    )
    picked = jnp.take(returned.reshape(expert_count * capacity, model_width), own_dest, axis=0)
    picked = picked.reshape(sub_rows, 2, model_width).astype(jnp.float32)
    routed_out = (
        picked[:, 0] * route_weights[:, 0:1] + picked[:, 1] * route_weights[:, 1:2]
    ).astype(jnp.bfloat16)
    return (mixed_rows, routed_out)


def solution(mesh):
    return jax.shard_map(
        shards,
        mesh=mesh,
        in_specs=(
            P("ep", "tp"),
            P("ep", "tp"),
            P("ep", "tp"),
            P("ep", "tp"),
            P("tp", None),
            P("ep", None),
            P("ep", None),
            P(("ep", "tp"), None),
            P("ep", None, "tp"),
            P("ep", None, "tp"),
            P("ep", "tp", None),
        ),
        out_specs=(P(("ep", "tp"), None), P(("ep", "tp"), None)),
        check_vma=False,
    )
```

profile of v0, /device:TPU:228, one launch (start us, length us, event | category | flops | bytes accessed | tf_op | source)
XLA Modules:
  0.0 330.9 jit_solution(5430103602426483478)
XLA Ops:
  11.9 21.6 %all_to_all.20 = bf16[32,2,4096]{2,1,0:T(2,128)(2,1)S(1)} all-to-all(bf16[32,2,4096]{2,1,0:T(2,128)(2,1)S(1)} %broadcast_select_fusion.1), channel_id=1, replica_groups=mesh['ep'=32,'tp'=8] {'ep'}, dimensions={0} | all-to-all | bytes 1048576 | tf_op jit(solution)/shard_map/all_to_all | solution.py:146
  35.8 34.8 %all-gather.5.cloned.1.call-done = bf16[32,16,4096]{2,0,1:T(8,128)(2,1)} async-done(((bf16[32,2,4096]{2,0,1:T(8,128)(2,1)}), bf16[32,16,4096]{2,0,1:T(8,128)(2,1)}) %all-gather.5.cloned.1.call-update) | async-done | bytes 4194320 | tf_op jit(solution)/shard_map/all_gather | solution.py:147
  70.6 3.6 %fusion.21 = f32[32,16,128]{2,0,1:T(8,128)S(1)} fusion(bf16[32,16,4096]{2,0,1:T(8,128)(2,1)} %all-gather.5.cloned.1.call-done, bf16[1,4096,128]{2,1,0:T(8,128)(2,1)S(1)} %copy-done.2), kind=kOutput, calls=%fused_computation.41 | convolution fusion | flops 536870912 | bytes 5505024 | tf_op jit(solution)/shard_map/rcd,df->rcf/dot_general | solution.py:99
  76.9 53.0 %all_to_all.21 = bf16[8,64,4096]{2,1,0:T(8,128)(2,1)} all-to-all(bf16[8,64,4096]{2,1,0:T(8,128)(2,1)S(1)} %bitcast.121), channel_id=1, replica_groups=mesh['ep'=32,'tp'=8] {'tp'}, dimensions={0} | all-to-all | bytes 8388608 | tf_op jit(solution)/shard_map/all_to_all | solution.py:26
  129.9 2.9 reduce_sum.65
  134.1 9.6 %all-to-all-start.3 = ((bf16[32,2,4096]{2,1,0:T(2,128)(2,1)}), bf16[32,2,4096]{2,1,0:T(2,128)(2,1)S(1)}, u32[]{:S(2)}, u32[]{:S(2)}) async-start(bf16[32,2,4096]{2,1,0:T(2,128)(2,1)} %reshape.292), calls=%async_computation.3 | async-start | bytes 1048576 | tf_op jit(solution)/shard_map/all_to_all | solution.py:158
  144.2 19.2 %all-to-all-done.3 = bf16[32,2,4096]{2,1,0:T(2,128)(2,1)S(1)} async-done(((bf16[32,2,4096]{2,1,0:T(2,128)(2,1)}), bf16[32,2,4096]{2,1,0:T(2,128)(2,1)S(1)}, u32[]{:S(2)}, u32[]{:S(2)}) %all-to-all-start.3) | async-done | bytes 524320 | tf_op jit(solution)/shard_map/all_to_all | solution.py:158
  164.5 20.7 %all-gather.3.cloned.1.call-done = bf16[4096,1032]{0,1:T(8,128)(2,1)} async-done(((bf16[128,1032]{0,1:T(8,128)(2,1)}), bf16[4096,1032]{0,1:T(8,128)(2,1)}) %all-gather.3.cloned.1.call-update) | async-done | bytes 8454160 | tf_op jit(solution)/shard_map/all_gather | solution.py:12
  185.3 6.0 %fusion.32 = (bf16[4096,512]{0,1:T(8,128)(2,1)}, bf16[4096,512]{0,1:T(8,128)(2,1)}) fusion(bf16[4096,1032]{0,1:T(8,128)(2,1)} %all-gather.3.cloned.1.call-done), kind=kLoop, calls=%fused_computation.81 | loop fusion | bytes 16777216 | tf_op jit(solution)/shard_map/slice | solution.py:14
  191.3 106.6 %while.13 = (s32[]{:T(128)}, f32[8,128,64]{1,2,0:T(8,128)S(1)}, f32[8,128]{1,0:T(8,128)S(1)}, s32[]{:T(128)}, s32[]{:T(128)}, /*index=5*/bf16[4096,512]{0,1:T(8,...) while((s32[]{:T(128)}, f32[8,128,64]{1,2,0:T(8,128)S(1)}, ...), condition=%wide.region_4.5_spmd.clone, body=%wide.region_0.4_spmd.clone.sunk | while | flops 219303552 | bytes 27235536 | solution.py:73
  193.0 2.4 fusion.56
  195.3 5.1 %fusion.57 = f32[8,128,4,128]{1,0,3,2:T(8,128)S(1)} fusion(f32[8,128,4,128]{1,3,2,0:T(8,128)S(1)} %bitcast.119), kind=kOutput, calls=%fused_computation.21.clone.1 | output fusion | flops 66584576 | bytes 4194304 | tf_op jit(solution)/shard_map/reduce-window
  201.0 3.4 %fusion.59 = bf16[8,128,512]{1,2,0:T(8,128)(2,1)S(1)} fusion(f32[8,128,4,128]{1,3,2,0:T(8,128)S(1)} %copy.90, f32[8,512,128]{2,1,0:T(8,128)S(1)} %get-tuple-element.183, f32[8,128]{1,0:T(8,128)S(1)} %get-tuple-element.201, f32[8,512]{1,0:T(8,128)S(1)} %convert_bitcast_fusion.2, pred[128,512]{0,1:T(8,128)(4,1)S(1)} %broadcast_compare_fusion.2), kind=kLoop, calls=%fused_computation.9.clone.1 | loop fusion | flops 12058624 | bytes 5328896 | tf_op jit(solution)/shard_map/while/body/convert_element_type | solution.py:61
  206.3 2.4 fusion.56
  208.6 5.1 %fusion.57 = f32[8,128,4,128]{1,0,3,2:T(8,128)S(1)} fusion(f32[8,128,4,128]{1,3,2,0:T(8,128)S(1)} %bitcast.119), kind=kOutput, calls=%fused_computation.21.clone.1 | output fusion | flops 66584576 | bytes 4194304 | tf_op jit(solution)/shard_map/reduce-window
  214.3 3.4 %fusion.59 = bf16[8,128,512]{1,2,0:T(8,128)(2,1)S(1)} fusion(f32[8,128,4,128]{1,3,2,0:T(8,128)S(1)} %copy.90, f32[8,512,128]{2,1,0:T(8,128)S(1)} %get-tuple-element.183, f32[8,128]{1,0:T(8,128)S(1)} %get-tuple-element.201, f32[8,512]{1,0:T(8,128)S(1)} %convert_bitcast_fusion.2, pred[128,512]{0,1:T(8,128)(4,1)S(1)} %broadcast_compare_fusion.2), kind=kLoop, calls=%fused_computation.9.clone.1 | loop fusion | flops 12058624 | bytes 5328896 | tf_op jit(solution)/shard_map/while/body/convert_element_type | solution.py:61
  222.0 5.1 %fusion.57 = f32[8,128,4,128]{1,0,3,2:T(8,128)S(1)} fusion(f32[8,128,4,128]{1,3,2,0:T(8,128)S(1)} %bitcast.119), kind=kOutput, calls=%fused_computation.21.clone.1 | output fusion | flops 66584576 | bytes 4194304 | tf_op jit(solution)/shard_map/reduce-window
  227.6 3.4 %fusion.59 = bf16[8,128,512]{1,2,0:T(8,128)(2,1)S(1)} fusion(f32[8,128,4,128]{1,3,2,0:T(8,128)S(1)} %copy.90, f32[8,512,128]{2,1,0:T(8,128)S(1)} %get-tuple-element.183, f32[8,128]{1,0:T(8,128)S(1)} %get-tuple-element.201, f32[8,512]{1,0:T(8,128)S(1)} %convert_bitcast_fusion.2, pred[128,512]{0,1:T(8,128)(4,1)S(1)} %broadcast_compare_fusion.2), kind=kLoop, calls=%fused_computation.9.clone.1 | loop fusion | flops 12058624 | bytes 5328896 | tf_op jit(solution)/shard_map/while/body/convert_element_type | solution.py:61
  232.9 2.4 fusion.56
  235.3 5.1 %fusion.57 = f32[8,128,4,128]{1,0,3,2:T(8,128)S(1)} fusion(f32[8,128,4,128]{1,3,2,0:T(8,128)S(1)} %bitcast.119), kind=kOutput, calls=%fused_computation.21.clone.1 | output fusion | flops 66584576 | bytes 4194304 | tf_op jit(solution)/shard_map/reduce-window
  240.9 3.4 %fusion.59 = bf16[8,128,512]{1,2,0:T(8,128)(2,1)S(1)} fusion(f32[8,128,4,128]{1,3,2,0:T(8,128)S(1)} %copy.90, f32[8,512,128]{2,1,0:T(8,128)S(1)} %get-tuple-element.183, f32[8,128]{1,0:T(8,128)S(1)} %get-tuple-element.201, f32[8,512]{1,0:T(8,128)S(1)} %convert_bitcast_fusion.2, pred[128,512]{0,1:T(8,128)(4,1)S(1)} %broadcast_compare_fusion.2), kind=kLoop, calls=%fused_computation.9.clone.1 | loop fusion | flops 12058624 | bytes 5328896 | tf_op jit(solution)/shard_map/while/body/convert_element_type | solution.py:61
  248.6 5.1 %fusion.57 = f32[8,128,4,128]{1,0,3,2:T(8,128)S(1)} fusion(f32[8,128,4,128]{1,3,2,0:T(8,128)S(1)} %bitcast.119), kind=kOutput, calls=%fused_computation.21.clone.1 | output fusion | flops 66584576 | bytes 4194304 | tf_op jit(solution)/shard_map/reduce-window
  254.2 3.4 %fusion.59 = bf16[8,128,512]{1,2,0:T(8,128)(2,1)S(1)} fusion(f32[8,128,4,128]{1,3,2,0:T(8,128)S(1)} %copy.90, f32[8,512,128]{2,1,0:T(8,128)S(1)} %get-tuple-element.183, f32[8,128]{1,0:T(8,128)S(1)} %get-tuple-element.201, f32[8,512]{1,0:T(8,128)S(1)} %convert_bitcast_fusion.2, pred[128,512]{0,1:T(8,128)(4,1)S(1)} %broadcast_compare_fusion.2), kind=kLoop, calls=%fused_computation.9.clone.1 | loop fusion | flops 12058624 | bytes 5328896 | tf_op jit(solution)/shard_map/while/body/convert_element_type | solution.py:61
  261.9 5.1 %fusion.57 = f32[8,128,4,128]{1,0,3,2:T(8,128)S(1)} fusion(f32[8,128,4,128]{1,3,2,0:T(8,128)S(1)} %bitcast.119), kind=kOutput, calls=%fused_computation.21.clone.1 | output fusion | flops 66584576 | bytes 4194304 | tf_op jit(solution)/shard_map/reduce-window
  267.5 3.4 %fusion.59 = bf16[8,128,512]{1,2,0:T(8,128)(2,1)S(1)} fusion(f32[8,128,4,128]{1,3,2,0:T(8,128)S(1)} %copy.90, f32[8,512,128]{2,1,0:T(8,128)S(1)} %get-tuple-element.183, f32[8,128]{1,0:T(8,128)S(1)} %get-tuple-element.201, f32[8,512]{1,0:T(8,128)S(1)} %convert_bitcast_fusion.2, pred[128,512]{0,1:T(8,128)(4,1)S(1)} %broadcast_compare_fusion.2), kind=kLoop, calls=%fused_computation.9.clone.1 | loop fusion | flops 12058624 | bytes 5328896 | tf_op jit(solution)/shard_map/while/body/convert_element_type | solution.py:61
  275.2 5.1 %fusion.57 = f32[8,128,4,128]{1,0,3,2:T(8,128)S(1)} fusion(f32[8,128,4,128]{1,3,2,0:T(8,128)S(1)} %bitcast.119), kind=kOutput, calls=%fused_computation.21.clone.1 | output fusion | flops 66584576 | bytes 4194304 | tf_op jit(solution)/shard_map/reduce-window
  280.8 3.4 %fusion.59 = bf16[8,128,512]{1,2,0:T(8,128)(2,1)S(1)} fusion(f32[8,128,4,128]{1,3,2,0:T(8,128)S(1)} %copy.90, f32[8,512,128]{2,1,0:T(8,128)S(1)} %get-tuple-element.183, f32[8,128]{1,0:T(8,128)S(1)} %get-tuple-element.201, f32[8,512]{1,0:T(8,128)S(1)} %convert_bitcast_fusion.2, pred[128,512]{0,1:T(8,128)(4,1)S(1)} %broadcast_compare_fusion.2), kind=kLoop, calls=%fused_computation.9.clone.1 | loop fusion | flops 12058624 | bytes 5328896 | tf_op jit(solution)/shard_map/while/body/convert_element_type | solution.py:61
  288.5 5.1 %fusion.57 = f32[8,128,4,128]{1,0,3,2:T(8,128)S(1)} fusion(f32[8,128,4,128]{1,3,2,0:T(8,128)S(1)} %bitcast.119), kind=kOutput, calls=%fused_computation.21.clone.1 | output fusion | flops 66584576 | bytes 4194304 | tf_op jit(solution)/shard_map/reduce-window
  294.1 3.4 %fusion.59 = bf16[8,128,512]{1,2,0:T(8,128)(2,1)S(1)} fusion(f32[8,128,4,128]{1,3,2,0:T(8,128)S(1)} %copy.90, f32[8,512,128]{2,1,0:T(8,128)S(1)} %get-tuple-element.183, f32[8,128]{1,0:T(8,128)S(1)} %get-tuple-element.201, f32[8,512]{1,0:T(8,128)S(1)} %convert_bitcast_fusion.2, pred[128,512]{0,1:T(8,128)(4,1)S(1)} %broadcast_compare_fusion.2), kind=kLoop, calls=%fused_computation.9.clone.1 | loop fusion | flops 12058624 | bytes 5328896 | tf_op jit(solution)/shard_map/while/body/convert_element_type | solution.py:61
  297.9 3.9 %convolution_convert_fusion.1 = bf16[128,4096]{1,0:T(8,128)(2,1)} fusion(bf16[128,512]{0,1:T(8,128)(2,1)S(1)} %bitcast.124, bf16[512,4096]{1,0:T(8,128)(2,1)} %param.17), kind=kOutput, calls=%fused_computation.36 | convolution fusion | flops 537395200 | bytes 5373952 | tf_op jit(solution)/shard_map/dot_general | solution.py:128
  301.9 5.4 %all-to-all-start = ((bf16[8,16,4096]{2,1,0:T(8,128)(2,1)}), bf16[8,16,4096]{2,1,0:T(8,128)(2,1)S(1)}, u32[]{:S(2)}, u32[]{:S(2)}) async-start(bf16[8,16,4096]{2,1,0:T(8,128)(2,1)} %bitcast.3), calls=%async_computation | async-start | bytes 2097152 | tf_op jit(solution)/shard_map/all_to_all | solution.py:26
  308.4 14.9 %all-to-all-done = bf16[8,16,4096]{2,1,0:T(8,128)(2,1)S(1)} async-done(((bf16[8,16,4096]{2,1,0:T(8,128)(2,1)}), bf16[8,16,4096]{2,1,0:T(8,128)(2,1)S(1)}, u32[]{:S(2)}, u32[]{:S(2)}) %all-to-all-start) | async-done | bytes 1048608 | tf_op jit(solution)/shard_map/all_to_all | solution.py:26
  (161 shorter events, 44.8 us)
Async XLA Ops:
  7.2 68.5 %copy-start = (bf16[1,128,4096]{2,1,0:T(8,128)(2,1)S(1)}, bf16[1,128,4096]{2,1,0:T(8,128)(2,1)}, u32[]{:S(2)}) copy-start(bf16[1,128,4096]{2,1,0:T(8,128)(2,1)} %param.23) | copy-start | bytes 3145732
  7.2 63.4 %all-gather.5.cloned.1.call-start = ((), (), s32[]{:S(2)}) async-start(), calls=%async_computation.5 | async-start | bytes 4718592 | tf_op jit(solution)/shard_map/all_gather | solution.py:147
  11.0 23.7 %copy-start.3 = (bf16[128,512]{1,0:T(8,128)(2,1)S(1)}, bf16[128,512]{1,0:T(8,128)(2,1)}, u32[]{:S(2)}) copy-start(bf16[128,512]{1,0:T(8,128)(2,1)} %param.14) | copy-start | bytes 393220
  11.0 23.9 %copy-start.4 = (bf16[128,512]{1,0:T(8,128)(2,1)S(1)}, bf16[128,512]{1,0:T(8,128)(2,1)}, u32[]{:S(2)}) copy-start(bf16[128,512]{1,0:T(8,128)(2,1)} %param.15) | copy-start | bytes 393220
  11.2 23.9 %copy-start.6 = (bf16[128,8]{0,1:T(8,128)(2,1)S(1)}, bf16[128,8]{0,1:T(8,128)(2,1)}, u32[]{:S(2)}) copy-start(bf16[128,8]{0,1:T(8,128)(2,1)} %param.16) | copy-start | bytes 6148
  11.9 58.6 %copy-start.2 = (bf16[1,4096,128]{2,1,0:T(8,128)(2,1)S(1)}, bf16[1,4096,128]{2,1,0:T(8,128)(2,1)}, u32[]{:S(2)}) copy-start(bf16[1,4096,128]{2,1,0:T(8,128)(2,1)} %param.21) | copy-start | bytes 3145732
  34.7 150.6 %all-gather.3.cloned.1.call-start = ((), (), s32[]{:S(2)}) async-start(), calls=%async_computation.4 | async-start | bytes 8718336 | tf_op jit(solution)/shard_map/all_gather | solution.py:12
  70.6 3.6 %copy-start.1 = (bf16[32,16,4096]{2,0,1:T(8,128)(2,1)S(1)}, bf16[32,16,4096]{2,0,1:T(8,128)(2,1)}, u32[]{:S(2)}) copy-start(bf16[32,16,4096]{2,0,1:T(8,128)(2,1)} %all-gather.5.cloned.1.call-done) | copy-start | bytes 12582916
  70.6 3.7 %copy-start.8 = (bf16[1,4096,128]{2,1,0:T(8,128)(2,1)S(1)}, bf16[1,4096,128]{2,1,0:T(8,128)(2,1)}, u32[]{:S(2)}) copy-start(bf16[1,4096,128]{2,1,0:T(8,128)(2,1)} %param.22) | copy-start | bytes 3145732
  132.9 11.1 %copy-start.5 = (bf16[128,512]{1,0:T(8,128)(2,1)S(1)}, bf16[128,512]{1,0:T(8,128)(2,1)}, u32[]{:S(2)}) copy-start(bf16[128,512]{1,0:T(8,128)(2,1)} %param.13) | copy-start | bytes 393220
  132.9 11.3 %copy-start.7 = (f32[16,2]{0,1:T(2,128)S(1)}, f32[16,2]{0,1:T(2,128)}, u32[]{:S(2)}) copy-start(f32[16,2]{0,1:T(2,128)} %param.20) | copy-start | bytes 388
  134.1 29.4 %all-to-all-start.3 = ((bf16[32,2,4096]{2,1,0:T(2,128)(2,1)}), bf16[32,2,4096]{2,1,0:T(2,128)(2,1)S(1)}, u32[]{:S(2)}, u32[]{:S(2)}) async-start(bf16[32,2,4096]{2,1,0:T(2,128)(2,1)} %reshape.292), calls=%async_computation.3 | async-start | bytes 1048576 | tf_op jit(solution)/shard_map/all_to_all | solution.py:158
  185.3 6.0 %slice-start = ((bf16[4096,1032]{0,1:T(8,128)(2,1)}), bf16[4096,8]{0,1:T(8,128)(2,1)S(1)}, s32[]{:S(2)}) async-start(bf16[4096,1032]{0,1:T(8,128)(2,1)} %all-gather.3.cloned.1.call-done), calls=%async_computation.6 | async-start | bytes 131072 | tf_op jit(solution)/shard_map/slice | solution.py:14
  301.9 21.4 %all-to-all-start = ((bf16[8,16,4096]{2,1,0:T(8,128)(2,1)}), bf16[8,16,4096]{2,1,0:T(8,128)(2,1)S(1)}, u32[]{:S(2)}, u32[]{:S(2)}) async-start(bf16[8,16,4096]{2,1,0:T(8,128)(2,1)} %bitcast.3), calls=%async_computation | async-start | bytes 2097152 | tf_op jit(solution)/shard_map/all_to_all | solution.py:26
Sparse Core Ops, SparseCore 0:
  34.8 35.6 all-gather.4
  73.0 112.2 all-gather.2
where the time goes:
time: 331 us
  waiting for transfers between devices  89.6 us (27%)
  other arithmetic  77.9 us (24%)
  blocking collectives  74.6 us (23%)
  matrix products  31.7 us (10%)
  local copies, waits for them, and re-layouts  26.4 us (8%)
  starting transfers between devices  15.1 us (5%)
  between operations  14.4 us (4%)
    all_to_all x1, blocking collectives, sent_and_summed(): lax.all_to_all(tiles, axis, split_axis=0, concat_axis=0, tiled=True)  53 us
    another operation x16, other arithmetic  40.5 us
    all_gather x1, waiting for transfers between devices, shards(): lax.all_gather(arrived, 'tp', axis=1, tiled=True)  34.8 us
    convert_element_type x8, other arithmetic, sweep_block(): jnp.where(strict, jnp.exp(jax.nn.log_sigmoid(scores) + suffix), 0.0)  27.2 us
    all_to_all x1, blocking collectives, shards(): lax.all_to_all(outgoing, 'ep', split_axis=0, concat_axis=0, tiled=True)  21.6 us
    all_gather x1, waiting for transfers between devices, sent_together(): lax.all_gather(both, axis, axis=dim, tiled=True)  20.7 us
    all_to_all x1, waiting for transfers between devices, shards(): lax.all_to_all(partial_value.reshape(expert_count, capacity, model_width)...  19.2 us
    dot_general x8, matrix products, sweep_block(): jnp.einsum('thd,shd->hts', query_rows, key_tile_block, preferred_element_...  19 us
  transfers between devices with their start and end apart: 4, of which 4 were waited for; matrix products, arithmetic and copies ran while one was open for 4% of the time, Pallas kernels for 0%

commit v1 on v0

--- a/solution.py
+++ b/solution.py
@@ -5,6 +5,14 @@
 
 HEAD = 64
 KEY_BLOCK = 512
+
+
+def gather_from_all(array, axis, dim):
+    length = lax.axis_size(axis)
+    repeats = [length if d == dim else 1 for d in range(array.ndim)]
+    return lax.all_to_all(
+        jnp.tile(array, repeats), axis, split_axis=dim, concat_axis=dim, tiled=True
+    )
 
 
 def sent_together(arrays, axis, dim, along):
@@ -144,7 +152,7 @@
         expert_count, capacity, model_width
     )
     arrived = lax.all_to_all(outgoing, "ep", split_axis=0, concat_axis=0, tiled=True)
-    hidden = expand(lax.all_gather(arrived, "tp", axis=1, tiled=True), gate_weight[0], up_weight[0])
+    hidden = expand(gather_from_all(arrived, "tp", 1), gate_weight[0], up_weight[0])
     unit_count = hidden.shape[2]
     ordered = jnp.transpose(
         hidden.reshape(expert_count, tp_count, capacity, unit_count), (1, 0, 2, 3)

time: 331 us -> 326 us (0.985)
  waiting for transfers between devices: 89.6 us -> 27.1 us
  blocking collectives: 74.6 us -> 131 us
    all_to_all x0 -> x1, blocking collectives: none -> 54.1 us  [gather_from_all(): lax.all_to_all(jnp.tile(array, repeats), axis, split_axis=dim, concat_axi...]
    all_gather x1 -> x0, waiting for transfers between devices: 34.8 us -> none  [shards(): lax.all_gather(arrived, 'tp', axis=1, tiled=True)]
    all_gather x1, waiting for transfers between devices: 20.7 us -> 0.02 us  [sent_together(): lax.all_gather(both, axis, axis=dim, tiled=True)]
    all_to_all x1, waiting for transfers between devices: 19.2 us -> 12.3 us  [shards(): lax.all_to_all(partial_value.reshape(expert_count, capacity, model_width)...]
  transfers between devices with their start and end apart: 4 -> 3, of which waited for: 4 -> 2; matrix products, arithmetic and copies ran while one was open for 4% -> 5% of each run, Pallas kernels for 0% -> 0%
where the time goes in v1:
time: 326 us; the launch traced here: 323 us
  blocking collectives  131 us (40%)
  other arithmetic  78.5 us (24%)
  matrix products  29.4 us (9%)
  local copies, waits for them, and re-layouts  27.8 us (9%)
  waiting for transfers between devices  27.1 us (8%)
  between operations  14.4 us (4%)
  starting transfers between devices  13.4 us (4%)
    all_to_all x1, blocking collectives, gather_from_all(): lax.all_to_all(jnp.tile(array, repeats), axis, split_axis=dim, concat_axi...  54.1 us
    all_to_all x1, blocking collectives, sent_and_summed(): lax.all_to_all(tiles, axis, split_axis=0, concat_axis=0, tiled=True)  53 us
    another operation x16, other arithmetic  40.5 us
    convert_element_type x8, other arithmetic, sweep_block(): jnp.where(strict, jnp.exp(jax.nn.log_sigmoid(scores) + suffix), 0.0)  27.2 us
    all_to_all x1, blocking collectives, shards(): lax.all_to_all(outgoing, 'ep', split_axis=0, concat_axis=0, tiled=True)  24.2 us
    dot_general x8, matrix products, sweep_block(): jnp.einsum('thd,shd->hts', query_rows, key_tile_block, preferred_element_...  19 us
    all_to_all x1, waiting for transfers between devices, sent_and_summed(): lax.all_to_all(tiles, axis, split_axis=0, concat_axis=0, tiled=True)  14.8 us
    all_to_all x1, waiting for transfers between devices, shards(): lax.all_to_all(partial_value.reshape(expert_count, capacity, model_width)...  12.3 us
  transfers between devices with their start and end apart: 3, of which 2 were waited for; matrix products, arithmetic and copies ran while one was open for 5% of the time, Pallas kernels for 0%

profile of v1, /device:TPU:228, one launch (start us, length us, event | category | flops | bytes accessed | tf_op | source)
XLA Modules:
  0.0 323.0 jit_solution(10118431513816423314)
XLA Ops:
  15.4 24.2 %all_to_all.25 = bf16[32,2,4096]{2,1,0:T(2,128)(2,1)S(1)} all-to-all(bf16[32,2,4096]{2,1,0:T(2,128)(2,1)S(1)} %broadcast_select_fusion.1), channel_id=1, replica_groups=mesh['ep'=32,'tp'=8] {'ep'}, dimensions={0} | all-to-all | bytes 1048576 | tf_op jit(solution)/shard_map/all_to_all | solution.py:154
  40.4 54.1 %all_to_all.26 = bf16[32,16,4096]{2,0,1:T(8,128)(2,1)S(1)} all-to-all(bf16[32,16,4096]{2,0,1:T(8,128)(2,1)S(1)} %bitcast.123), channel_id=1, replica_groups=mesh['ep'=32,'tp'=8] {'tp'}, dimensions={1} | all-to-all | bytes 8388608 | tf_op jit(solution)/shard_map/all_to_all | solution.py:13
  98.5 53.0 %all_to_all.27 = bf16[8,64,4096]{2,1,0:T(8,128)(2,1)} all-to-all(bf16[8,64,4096]{2,1,0:T(8,128)(2,1)S(1)} %bitcast.122), channel_id=1, replica_groups=mesh['ep'=32,'tp'=8] {'tp'}, dimensions={0} | all-to-all | bytes 8388608 | tf_op jit(solution)/shard_map/all_to_all | solution.py:34
  151.4 2.9 reduce_sum.65
  155.6 9.8 %all-to-all-start.4 = ((bf16[32,2,4096]{2,1,0:T(2,128)(2,1)}), bf16[32,2,4096]{2,1,0:T(2,128)(2,1)S(1)}, u32[]{:S(2)}, u32[]{:S(2)}) async-start(bf16[32,2,4096]{2,1,0:T(2,128)(2,1)} %reshape.296), calls=%async_computation.4 | async-start | bytes 1048576 | tf_op jit(solution)/shard_map/all_to_all | solution.py:166
  165.9 12.3 %all-to-all-done.4 = bf16[32,2,4096]{2,1,0:T(2,128)(2,1)S(1)} async-done(((bf16[32,2,4096]{2,1,0:T(2,128)(2,1)}), bf16[32,2,4096]{2,1,0:T(2,128)(2,1)S(1)}, u32[]{:S(2)}, u32[]{:S(2)}) %all-to-all-start.4) | async-done | bytes 524320 | tf_op jit(solution)/shard_map/all_to_all | solution.py:166
  179.3 6.0 %fusion.32 = (bf16[4096,512]{0,1:T(8,128)(2,1)}, bf16[4096,512]{0,1:T(8,128)(2,1)}) fusion(bf16[4096,1032]{0,1:T(8,128)(2,1)} %all-gather.2.cloned.1.call-done), kind=kLoop, calls=%fused_computation.81 | loop fusion | bytes 16777216 | tf_op jit(solution)/shard_map/slice | solution.py:22
  185.3 106.6 %while.13 = (s32[]{:T(128)}, f32[8,128,64]{1,2,0:T(8,128)S(1)}, f32[8,128]{1,0:T(8,128)S(1)}, s32[]{:T(128)}, s32[]{:T(128)}, /*index=5*/bf16[4096,512]{0,1:T(8,...) while((s32[]{:T(128)}, f32[8,128,64]{1,2,0:T(8,128)S(1)}, ...), condition=%wide.region_4.5_spmd.clone, body=%wide.region_0.4_spmd.clone.sunk | while | flops 219303552 | bytes 27235536 | solution.py:81
  187.0 2.4 fusion.56
  189.4 5.1 %fusion.57 = f32[8,128,4,128]{1,0,3,2:T(8,128)S(1)} fusion(f32[8,128,4,128]{1,3,2,0:T(8,128)S(1)} %bitcast.120), kind=kOutput, calls=%fused_computation.21.clone.1 | output fusion | flops 66584576 | bytes 4194304 | tf_op jit(solution)/shard_map/reduce-window
  195.1 3.4 %fusion.59 = bf16[8,128,512]{1,2,0:T(8,128)(2,1)S(1)} fusion(f32[8,128,4,128]{1,3,2,0:T(8,128)S(1)} %copy.77, f32[8,512,128]{2,1,0:T(8,128)S(1)} %get-tuple-element.183, f32[8,128]{1,0:T(8,128)S(1)} %get-tuple-element.201, f32[8,512]{1,0:T(8,128)S(1)} %convert_bitcast_fusion.2, pred[128,512]{0,1:T(8,128)(4,1)S(1)} %broadcast_compare_fusion.2), kind=kLoop, calls=%fused_computation.9.clone.1 | loop fusion | flops 12058624 | bytes 5328896 | tf_op jit(solution)/shard_map/while/body/convert_element_type | solution.py:69
  200.3 2.4 fusion.56
  202.7 5.1 %fusion.57 = f32[8,128,4,128]{1,0,3,2:T(8,128)S(1)} fusion(f32[8,128,4,128]{1,3,2,0:T(8,128)S(1)} %bitcast.120), kind=kOutput, calls=%fused_computation.21.clone.1 | output fusion | flops 66584576 | bytes 4194304 | tf_op jit(solution)/shard_map/reduce-window
  208.4 3.4 %fusion.59 = bf16[8,128,512]{1,2,0:T(8,128)(2,1)S(1)} fusion(f32[8,128,4,128]{1,3,2,0:T(8,128)S(1)} %copy.77, f32[8,512,128]{2,1,0:T(8,128)S(1)} %get-tuple-element.183, f32[8,128]{1,0:T(8,128)S(1)} %get-tuple-element.201, f32[8,512]{1,0:T(8,128)S(1)} %convert_bitcast_fusion.2, pred[128,512]{0,1:T(8,128)(4,1)S(1)} %broadcast_compare_fusion.2), kind=kLoop, calls=%fused_computation.9.clone.1 | loop fusion | flops 12058624 | bytes 5328896 | tf_op jit(solution)/shard_map/while/body/convert_element_type | solution.py:69
  213.6 2.4 fusion.56
  216.0 5.1 %fusion.57 = f32[8,128,4,128]{1,0,3,2:T(8,128)S(1)} fusion(f32[8,128,4,128]{1,3,2,0:T(8,128)S(1)} %bitcast.120), kind=kOutput, calls=%fused_computation.21.clone.1 | output fusion | flops 66584576 | bytes 4194304 | tf_op jit(solution)/shard_map/reduce-window
  221.7 3.4 %fusion.59 = bf16[8,128,512]{1,2,0:T(8,128)(2,1)S(1)} fusion(f32[8,128,4,128]{1,3,2,0:T(8,128)S(1)} %copy.77, f32[8,512,128]{2,1,0:T(8,128)S(1)} %get-tuple-element.183, f32[8,128]{1,0:T(8,128)S(1)} %get-tuple-element.201, f32[8,512]{1,0:T(8,128)S(1)} %convert_bitcast_fusion.2, pred[128,512]{0,1:T(8,128)(4,1)S(1)} %broadcast_compare_fusion.2), kind=kLoop, calls=%fused_computation.9.clone.1 | loop fusion | flops 12058624 | bytes 5328896 | tf_op jit(solution)/shard_map/while/body/convert_element_type | solution.py:69
  229.3 5.1 %fusion.57 = f32[8,128,4,128]{1,0,3,2:T(8,128)S(1)} fusion(f32[8,128,4,128]{1,3,2,0:T(8,128)S(1)} %bitcast.120), kind=kOutput, calls=%fused_computation.21.clone.1 | output fusion | flops 66584576 | bytes 4194304 | tf_op jit(solution)/shard_map/reduce-window
  235.0 3.4 %fusion.59 = bf16[8,128,512]{1,2,0:T(8,128)(2,1)S(1)} fusion(f32[8,128,4,128]{1,3,2,0:T(8,128)S(1)} %copy.77, f32[8,512,128]{2,1,0:T(8,128)S(1)} %get-tuple-element.183, f32[8,128]{1,0:T(8,128)S(1)} %get-tuple-element.201, f32[8,512]{1,0:T(8,128)S(1)} %convert_bitcast_fusion.2, pred[128,512]{0,1:T(8,128)(4,1)S(1)} %broadcast_compare_fusion.2), kind=kLoop, calls=%fused_computation.9.clone.1 | loop fusion | flops 12058624 | bytes 5328896 | tf_op jit(solution)/shard_map/while/body/convert_element_type | solution.py:69
  242.6 5.1 %fusion.57 = f32[8,128,4,128]{1,0,3,2:T(8,128)S(1)} fusion(f32[8,128,4,128]{1,3,2,0:T(8,128)S(1)} %bitcast.120), kind=kOutput, calls=%fused_computation.21.clone.1 | output fusion | flops 66584576 | bytes 4194304 | tf_op jit(solution)/shard_map/reduce-window
  248.3 3.4 %fusion.59 = bf16[8,128,512]{1,2,0:T(8,128)(2,1)S(1)} fusion(f32[8,128,4,128]{1,3,2,0:T(8,128)S(1)} %copy.77, f32[8,512,128]{2,1,0:T(8,128)S(1)} %get-tuple-element.183, f32[8,128]{1,0:T(8,128)S(1)} %get-tuple-element.201, f32[8,512]{1,0:T(8,128)S(1)} %convert_bitcast_fusion.2, pred[128,512]{0,1:T(8,128)(4,1)S(1)} %broadcast_compare_fusion.2), kind=kLoop, calls=%fused_computation.9.clone.1 | loop fusion | flops 12058624 | bytes 5328896 | tf_op jit(solution)/shard_map/while/body/convert_element_type | solution.py:69
  253.5 2.4 fusion.56
  255.9 5.1 %fusion.57 = f32[8,128,4,128]{1,0,3,2:T(8,128)S(1)} fusion(f32[8,128,4,128]{1,3,2,0:T(8,128)S(1)} %bitcast.120), kind=kOutput, calls=%fused_computation.21.clone.1 | output fusion | flops 66584576 | bytes 4194304 | tf_op jit(solution)/shard_map/reduce-window
  261.6 3.4 %fusion.59 = bf16[8,128,512]{1,2,0:T(8,128)(2,1)S(1)} fusion(f32[8,128,4,128]{1,3,2,0:T(8,128)S(1)} %copy.77, f32[8,512,128]{2,1,0:T(8,128)S(1)} %get-tuple-element.183, f32[8,128]{1,0:T(8,128)S(1)} %get-tuple-element.201, f32[8,512]{1,0:T(8,128)S(1)} %convert_bitcast_fusion.2, pred[128,512]{0,1:T(8,128)(4,1)S(1)} %broadcast_compare_fusion.2), kind=kLoop, calls=%fused_computation.9.clone.1 | loop fusion | flops 12058624 | bytes 5328896 | tf_op jit(solution)/shard_map/while/body/convert_element_type | solution.py:69
  266.8 2.4 fusion.56
  269.2 5.1 %fusion.57 = f32[8,128,4,128]{1,0,3,2:T(8,128)S(1)} fusion(f32[8,128,4,128]{1,3,2,0:T(8,128)S(1)} %bitcast.120), kind=kOutput, calls=%fused_computation.21.clone.1 | output fusion | flops 66584576 | bytes 4194304 | tf_op jit(solution)/shard_map/reduce-window
  274.9 3.4 %fusion.59 = bf16[8,128,512]{1,2,0:T(8,128)(2,1)S(1)} fusion(f32[8,128,4,128]{1,3,2,0:T(8,128)S(1)} %copy.77, f32[8,512,128]{2,1,0:T(8,128)S(1)} %get-tuple-element.183, f32[8,128]{1,0:T(8,128)S(1)} %get-tuple-element.201, f32[8,512]{1,0:T(8,128)S(1)} %convert_bitcast_fusion.2, pred[128,512]{0,1:T(8,128)(4,1)S(1)} %broadcast_compare_fusion.2), kind=kLoop, calls=%fused_computation.9.clone.1 | loop fusion | flops 12058624 | bytes 5328896 | tf_op jit(solution)/shard_map/while/body/convert_element_type | solution.py:69
  282.5 5.1 %fusion.57 = f32[8,128,4,128]{1,0,3,2:T(8,128)S(1)} fusion(f32[8,128,4,128]{1,3,2,0:T(8,128)S(1)} %bitcast.120), kind=kOutput, calls=%fused_computation.21.clone.1 | output fusion | flops 66584576 | bytes 4194304 | tf_op jit(solution)/shard_map/reduce-window
  288.2 3.4 %fusion.59 = bf16[8,128,512]{1,2,0:T(8,128)(2,1)S(1)} fusion(f32[8,128,4,128]{1,3,2,0:T(8,128)S(1)} %copy.77, f32[8,512,128]{2,1,0:T(8,128)S(1)} %get-tuple-element.183, f32[8,128]{1,0:T(8,128)S(1)} %get-tuple-element.201, f32[8,512]{1,0:T(8,128)S(1)} %convert_bitcast_fusion.2, pred[128,512]{0,1:T(8,128)(4,1)S(1)} %broadcast_compare_fusion.2), kind=kLoop, calls=%fused_computation.9.clone.1 | loop fusion | flops 12058624 | bytes 5328896 | tf_op jit(solution)/shard_map/while/body/convert_element_type | solution.py:69
  292.0 3.9 %convolution_convert_fusion.1 = bf16[128,4096]{1,0:T(8,128)(2,1)} fusion(bf16[128,512]{0,1:T(8,128)(2,1)S(1)} %bitcast.126, bf16[512,4096]{1,0:T(8,128)(2,1)} %param.17), kind=kOutput, calls=%fused_computation.36 | convolution fusion | flops 537395200 | bytes 5373952 | tf_op jit(solution)/shard_map/dot_general | solution.py:136
  295.9 3.6 %all-to-all-start = ((bf16[8,16,4096]{2,1,0:T(8,128)(2,1)}), bf16[8,16,4096]{2,1,0:T(8,128)(2,1)S(1)}, u32[]{:S(2)}, u32[]{:S(2)}) async-start(bf16[8,16,4096]{2,1,0:T(8,128)(2,1)} %bitcast.3), calls=%async_computation | async-start | bytes 2097152 | tf_op jit(solution)/shard_map/all_to_all | solution.py:34
  300.6 14.8 %all-to-all-done = bf16[8,16,4096]{2,1,0:T(8,128)(2,1)S(1)} async-done(((bf16[8,16,4096]{2,1,0:T(8,128)(2,1)}), bf16[8,16,4096]{2,1,0:T(8,128)(2,1)S(1)}, u32[]{:S(2)}, u32[]{:S(2)}) %all-to-all-start) | async-done | bytes 1048608 | tf_op jit(solution)/shard_map/all_to_all | solution.py:34
  (152 shorter events, 43.3 us)
Async XLA Ops:
  7.2 90.0 %copy-start = (bf16[1,128,4096]{2,1,0:T(8,128)(2,1)S(1)}, bf16[1,128,4096]{2,1,0:T(8,128)(2,1)}, u32[]{:S(2)}) copy-start(bf16[1,128,4096]{2,1,0:T(8,128)(2,1)} %param.23) | copy-start | bytes 3145732
  7.2 172.1 %all-gather.2.cloned.1.call-start = ((), (), s32[]{:S(2)}) async-start(), calls=%async_computation.5 | async-start | bytes 8718336 | tf_op jit(solution)/shard_map/all_gather | solution.py:20
  40.4 54.1 %copy-start.1 = (bf16[1,4096,128]{2,1,0:T(8,128)(2,1)S(1)}, bf16[1,4096,128]{2,1,0:T(8,128)(2,1)}, u32[]{:S(2)}) copy-start(bf16[1,4096,128]{2,1,0:T(8,128)(2,1)} %param.21) | copy-start | bytes 3145732
  94.6 1.3 copy-start.4
  154.4 11.3 %copy-start.2 = (bf16[128,512]{1,0:T(8,128)(2,1)S(1)}, bf16[128,512]{1,0:T(8,128)(2,1)}, u32[]{:S(2)}) copy-start(bf16[128,512]{1,0:T(8,128)(2,1)} %param.13) | copy-start | bytes 393220
  154.4 11.5 %copy-start.3 = (f32[16,2]{0,1:T(2,128)S(1)}, f32[16,2]{0,1:T(2,128)}, u32[]{:S(2)}) copy-start(f32[16,2]{0,1:T(2,128)} %param.20) | copy-start | bytes 388
  155.6 22.6 %all-to-all-start.4 = ((bf16[32,2,4096]{2,1,0:T(2,128)(2,1)}), bf16[32,2,4096]{2,1,0:T(2,128)(2,1)S(1)}, u32[]{:S(2)}, u32[]{:S(2)}) async-start(bf16[32,2,4096]{2,1,0:T(2,128)(2,1)} %reshape.296), calls=%async_computation.4 | async-start | bytes 1048576 | tf_op jit(solution)/shard_map/all_to_all | solution.py:166
  179.3 6.0 %slice-start = ((bf16[4096,1032]{0,1:T(8,128)(2,1)}), bf16[4096,8]{0,1:T(8,128)(2,1)S(1)}, s32[]{:S(2)}) async-start(bf16[4096,1032]{0,1:T(8,128)(2,1)} %all-gather.2.cloned.1.call-done), calls=%async_computation.6 | async-start | bytes 131072 | tf_op jit(solution)/shard_map/slice | solution.py:22
  295.9 19.4 %all-to-all-start = ((bf16[8,16,4096]{2,1,0:T(8,128)(2,1)}), bf16[8,16,4096]{2,1,0:T(8,128)(2,1)S(1)}, u32[]{:S(2)}, u32[]{:S(2)}) async-start(bf16[8,16,4096]{2,1,0:T(8,128)(2,1)} %bitcast.3), calls=%async_computation | async-start | bytes 2097152 | tf_op jit(solution)/shard_map/all_to_all | solution.py:34
Sparse Core Ops, SparseCore 0:
  10.9 108.6 all-gather.1
